TPU v7x, 512 devices: a whole 4x4x16 slice. The times are simulated.
512 devices in a mesh: sp: 32 (over z, core), tp: 16 (over y, x).
Axes of the slice: x: 4, y: 4, z: 16, core: 2. Of those that a mesh axis runs over, the one named last changes fastest.
Arguments:
- residual: bfloat16 [8192, 4096], P('sp', 'tp'), may hold values from -6 to 6
- pool_in: bfloat16 [8192, 2048], P('sp', 'tp'), may hold values from -6 to 6
- docs: int32 [8192], P('sp'), may hold values from 0 to 15, never falling along the last dimension, each value on 1 to 1024 neighbouring positions
- pool_weight: bfloat16 [16, 128, 128], P('tp'), may hold values from -0.5 to 0.5
- pool_gain: float32 [2048], P('tp'), may hold values from 0.1 to 1.9
- out_weight: bfloat16 [2048, 4096], P(None, 'tp'), may hold values from -0.125 to 0.125
- norm_gain: float32 [4096], replicated, may hold values from 0.1 to 1.9
- routes: int32 [8192, 2], P('sp'), may hold values from 0 to 31, all different within a row; in each aligned block of 256 rows (0 to 255, 256 to 511, ...) at most 24 rows name the same one
- route_weights: float32 [8192, 2], P('sp'), may hold values from 0.25 to 1
- w_gate: bfloat16 [32, 4096, 2048], P('sp', None, 'tp'), may hold values from -0.09375 to 0.09375
- w_up: bfloat16 [32, 4096, 2048], P('sp', None, 'tp'), may hold values from -0.09375 to 0.09375
- w_down: bfloat16 [32, 2048, 4096], P('sp', None, 'tp'), may hold values from -0.125 to 0.125
Outputs:
- layer_out: bfloat16 [8192, 4096], P('sp', 'tp')
Inputs may be any that keep to these rules, and one draw needn't show every extreme that they name: `docs`: document numbers never fall along the sequence; each document has at most 1024 positions. `routes`: each token names 2 different experts; among the tokens of one index of sp (aligned blocks of 256 rows) no expert is named more than 24 times, a bound that some block reaches.
All inputs are finite; a program needn't handle non-finite values.
Results may differ from a plain program's by a relative error of at most 0.012.
Values may be sent and summed in bfloat16 or wider, within the bound.
No kernel may reach another device: no remote copies, remote signals or barrier semaphores. Data moves between devices by JAX's collectives and lax.ppermute only.
A program may use at most 64 MiB of HBM per device.

v0:
```python
import functools

import jax
import jax.numpy as jnp
from jax import lax
from jax.sharding import Mesh
from jax.sharding import PartitionSpec as P

GD = 128
TOPK = 2
EXP_DEV = 1
TP = ("tp_0", "tp_1")


EPS = 1e-06


def shifted_2(shard, axis, by):
    size = lax.axis_size(axis)
    pairs = [(i, i + by) for i in range(size) if 0 <= i + by < size]
    return lax.ppermute(shard, axis, pairs)


def sent_to_all(shard, axis):
    size = lax.axis_size(axis)
    return lax.all_to_all(
        jnp.broadcast_to(shard[None], (size, *shard.shape)), axis, 0, 0, tiled=True
    )


def laid_out(parts, dim):
    shape = list(parts.shape[1:])
    shape[dim] *= parts.shape[0]
    return jnp.moveaxis(parts, 0, dim).reshape(shape)


def collect(shard, axis, dim):
    parts = sent_to_all(shard, axis)
    return laid_out(parts, dim)


def by_axis(shard, axes):
    return functools.reduce(lax.psum, axes, shard)


def whole_of(shard, axes, dim):
    whole = shard
    for number in range(len(axes) - 1, -1, -1):
        whole = lax.all_gather(whole, axes[number], axis=dim, tiled=True)
    return whole


def shards(
    residual,
    pool_in,
    docs,
    pool_weight,
    pool_gain,
    out_weight,
    norm_gain,
    routes,
    route_weights,
    w_gate,
    w_up,
    w_down,
):
    length = pool_in.shape[0]
    width_loc = pool_in.shape[1]
    sp_index = lax.axis_index("sp")
    tp_index = lax.axis_index(TP)
    n_sp = lax.axis_size("sp")
    n_tp = lax.axis_size(TP)
    reach = 15
    prev_rows, prev_docs = shifted_2(
        (pool_in[length - reach :], docs[length - reach :].astype(jnp.bfloat16)), "sp", 1
    )
    extended = jnp.concatenate([prev_rows, pool_in], axis=0).astype(jnp.float32)
    ext_docs = jnp.concatenate([prev_docs.astype(jnp.float32), docs.astype(jnp.float32)])
    own_docs = docs.astype(jnp.float32)
    places = sp_index * length + jnp.arange(length)
    groups_loc = width_loc // GD
    group_of = tp_index * groups_loc + jnp.arange(width_loc) // GD
    span = 2 ** (1 + group_of % 4)
    totals = jnp.zeros((length, width_loc), jnp.float32)
    counts = jnp.zeros((length, width_loc), jnp.float32)
    for offset in range(16):
        shifted = extended[reach - offset : reach - offset + length]
        prior = ext_docs[reach - offset : reach - offset + length]
        same = ((places >= offset) & (prior == own_docs)).astype(jnp.float32)[:, None]
        weight = same * (offset < span).astype(jnp.float32)[None, :]
        totals = totals + weight * shifted
        counts = counts + weight
    diff = (totals / counts - extended[reach:]).astype(jnp.bfloat16)
    mixed = jnp.einsum(
        "tgc,gcd->tgd",
        diff.reshape(length, groups_loc, GD),
        pool_weight,
        preferred_element_type=jnp.float32,
    )
    pooled = (mixed.reshape(length, width_loc) * pool_gain).astype(jnp.bfloat16)
    block = out_weight
    proj = jnp.dot(collect(pooled, TP, 1), block, preferred_element_type=jnp.float32)
    updated = (residual.astype(jnp.float32) + proj).astype(jnp.bfloat16)
    upf = updated.astype(jnp.float32)
    cols = residual.shape[1]
    model_width = cols * n_tp
    experts = n_sp * EXP_DEV
    slots_cap = length * TOPK * 3 // (2 * experts)
    ids = routes.reshape(-1)
    onehot = (ids[:, None] == jnp.arange(experts)[None, :]).astype(jnp.int32)
    rank = jnp.sum(onehot * (jnp.cumsum(onehot, axis=0) - 1), axis=1)
    slot = ids * slots_cap + rank
    source = jnp.arange(length * TOPK) // TOPK
    squares = by_axis(jnp.sum(upf * upf, axis=1), TP)
    gain_cols = lax.dynamic_slice_in_dim(norm_gain, tp_index * cols, cols, 0)
    normed = (upf * lax.rsqrt(squares / model_width + EPS)[:, None] * gain_cols).astype(
        jnp.bfloat16
    )
    send = jnp.zeros((experts * slots_cap, cols), jnp.bfloat16).at[slot].set(normed[source])
    arrived = lax.all_to_all(
        send.reshape(experts, slots_cap, cols), "sp", split_axis=0, concat_axis=0, tiled=True
    )
    part_rows = arrived.reshape(-1, cols)
    piece = lax.all_gather(part_rows, TP, axis=1, tiled=True)
    gate_block = w_gate[0]
    up_block = w_up[0]
    gate = jnp.dot(piece, gate_block, preferred_element_type=jnp.float32)
    up = jnp.dot(piece, up_block, preferred_element_type=jnp.float32)
    act = (jax.nn.silu(gate) * up).astype(jnp.bfloat16)
    block = w_down[0]
    produced = jnp.dot(whole_of(act, TP, 1), block, preferred_element_type=jnp.float32).astype(
        jnp.bfloat16
    )
    returned = lax.all_to_all(
        produced.reshape(n_sp, slots_cap, cols), "sp", split_axis=0, concat_axis=0, tiled=True
    )
    picked = returned.reshape(-1, cols)[slot].reshape(length, TOPK, cols)
    combined = upf + jnp.sum(route_weights[:, :, None] * picked.astype(jnp.float32), axis=1)
    return combined.astype(jnp.bfloat16)


def solution(mesh):
    torus = Mesh(mesh.devices.reshape(mesh.shape["sp"], 4, 4), ("sp", "tp_0", "tp_1"))
    in_specs = (
        P("sp", TP),
        P("sp", TP),
        P("sp"),
        P(TP, None, None),
        P(TP),
        P(None, TP),
        P(),
        P("sp", None),
        P("sp", None),
        P("sp", None, TP),
        P("sp", None, TP),
        P("sp", None, TP),
    )
    out_specs = P("sp", TP)
    return jax.shard_map(
        shards, mesh=torus, in_specs=in_specs, out_specs=out_specs, check_vma=False
    )
```

profile of v0, /device:TPU:1, one launch (start us, length us, event | category | flops | bytes accessed | tf_op | source)
XLA Modules:
  0.0 306.7 jit_solution(17806507090641942363)
XLA Ops:
  6.5 0.8 fusion.37
  7.4 4.9 %collective-permute-start.1 = (bf16[15]{0:T(256)(128)(2,1)S(1)}, bf16[15]{0:T(256)(128)(2,1)S(1)}, u32[]{:S(2)}, u32[]{:S(2)}) collective-permute-start(bf16[15]{0:T(256)(128)(2,1)S(1)} %slice.109), channel_id=1, source_target_pairs={{0,16},{16,32},{32,48},{48,64},{64,80},{80,96},{96,112},{112,128},... | collective-permute-start | bytes 98 | tf_op jit(solution)/shard_map/ppermute | solution.py:21
  12.3 0.7 slice.107
  13.0 1.9 collective-permute-start
  15.2 0.8 copy.30
  16.3 0.8 and_convert_fusion.14
  17.0 1.1 collective-permute-done
  18.2 0.9 maximum_convert_fusion
  19.0 1.9 fusion.3
  21.0 1.1 broadcast_in_dim.8
  22.1 5.6 %all-to-all-start = ((bf16[16,256,128]{1,2,0:T(8,128)(2,1)}), bf16[16,256,128]{1,2,0:T(8,128)(2,1)S(1)}, u32[]{:S(2)}, u32[]{:S(2)}) async-start(bf16[16,256,128]{1,2,0:T(8,128)(2,1)} %broadcast_in_dim.8), calls=%async_computation | async-start | bytes 2097152 | tf_op jit(solution)/shard_map/all_to_all | solution.py:26
  28.0 1.2 reduce-window.6
  29.2 0.2 slice_reduce_fusion
  29.7 0.8 dynamic_slice.3
  30.6 13.3 %all-to-all-done = bf16[16,256,128]{1,2,0:T(8,128)(2,1)S(1)} async-done(((bf16[16,256,128]{1,2,0:T(8,128)(2,1)}), bf16[16,256,128]{1,2,0:T(8,128)(2,1)S(1)}, u32[]{:S(2)}, u32[]{:S(2)}) %all-to-all-start) | async-done | bytes 1048608 | tf_op jit(solution)/shard_map/all_to_all | solution.py:26
  43.9 1.9 multiply_reduce_fusion.1
  45.8 6.6 %psum.14 = f32[256]{0:T(256)S(1)} all-reduce(f32[256]{0:T(256)S(1)} %get-tuple-element.23), channel_id=1, replica_groups=mesh['sp'=32,'tp_0'=4,'tp_1'=4] {'tp_0'}, use_global_device_ids=true, to_apply=%region_4.5 | all-reduce | flops 256 | bytes 2048 | tf_op jit(solution)/shard_map/psum | solution.py:43
  52.4 6.7 %psum.15 = f32[256]{0:T(256)S(1)} all-reduce(f32[256]{0:T(256)S(1)} %psum.14), channel_id=1, replica_groups=mesh['sp'=32,'tp_0'=4,'tp_1'=4] {'tp_1'}, use_global_device_ids=true, to_apply=%region_5.6 | all-reduce | flops 256 | bytes 2048 | tf_op jit(solution)/shard_map/psum | solution.py:43
  59.3 3.9 %scatter_custom_fusion = bf16[768,256]{1,0:T(8,128)(2,1)S(1)} fusion(s32[512]{0:T(512)S(1)} %bitcast.46, bf16[256,256]{1,0:T(8,128)(2,1)S(1)} %copy.33, s32[1024]{0:T(1024)S(1)} %pad_clamp_fusion.1, bf16[]{:T(256)} %constant.166.clone.1), kind=kCustom, calls=%fused_computation.16 | custom fusion | bytes 393218 | tf_op jit(solution)/shard_map/scatter | solution.py:119
  63.2 48.2 %all_to_all.15 = bf16[32,24,256]{2,1,0:T(8,128)(2,1)} all-to-all(bf16[32,24,256]{2,1,0:T(8,128)(2,1)S(1)} %bitcast.44), channel_id=1, replica_groups=mesh['sp'=32,'tp_0'=4,'tp_1'=4] {'sp'}, dimensions={0} | all-to-all | bytes 786432 | tf_op jit(solution)/shard_map/all_to_all | solution.py:120
  111.5 68.2 %all-gather.3.cloned.1.call-done = bf16[768,4096]{1,0:T(8,128)(2,1)} async-done(((bf16[768,256]{1,0:T(8,128)(2,1)}), bf16[768,4096]{1,0:T(8,128)(2,1)}) %all-gather.3.cloned.1.call-update) | async-done | bytes 6291472 | tf_op jit(solution)/shard_map/all_gather | solution.py:124
  179.8 5.0 %fusion.6 = f32[768,128]{1,0:T(8,128)S(1)} fusion(bf16[768,4096]{1,0:T(8,128)(2,1)} %all-gather.3.cloned.1.call-done, bf16[1,4096,128]{2,1,0:T(8,128)(2,1)} %param.21), kind=kOutput, calls=%fused_computation.13 | convolution fusion | flops 805306368 | bytes 7733248 | tf_op jit(solution)/shard_map/dot_general | solution.py:127
  184.7 1.8 fusion
  186.6 15.7 %all_gather.10 = bf16[768,512]{1,0:T(8,128)(2,1)} all-gather(bf16[768,128]{1,0:T(8,128)(2,1)S(1)} %fusion), channel_id=1, replica_groups=mesh['sp'=32,'tp_0'=4,'tp_1'=4] {'tp_1'}, dimensions={1}, use_global_device_ids=true | all-gather | bytes 983040 | tf_op jit(solution)/shard_map/all_gather | solution.py:49
  202.3 49.1 %all-gather.5.cloned.1.call-done = bf16[768,2048]{1,0:T(8,128)(2,1)} async-done(((bf16[768,512]{1,0:T(8,128)(2,1)}), bf16[768,2048]{1,0:T(8,128)(2,1)}) %all-gather.5.cloned.1.call-update) | async-done | bytes 3145744 | tf_op jit(solution)/shard_map/all_gather | solution.py:49
  251.4 3.6 %convolution_convert_fusion = bf16[768,256]{1,0:T(8,128)(2,1)} fusion(bf16[768,2048]{1,0:T(8,128)(2,1)} %all-gather.5.cloned.1.call-done, bf16[1,2048,256]{2,1,0:T(8,128)(2,1)S(1)} %copy-done), kind=kOutput, calls=%fused_computation.3 | convolution fusion | flops 805502976 | bytes 4587520 | tf_op jit(solution)/shard_map/dot_general | solution.py:131
  255.1 13.2 %all-to-all-start.2 = ((bf16[32,24,256]{2,1,0:T(8,128)(2,1)}), bf16[32,24,256]{2,1,0:T(8,128)(2,1)S(1)}, u32[]{:S(2)}, u32[]{:S(2)}) async-start(bf16[32,24,256]{2,1,0:T(8,128)(2,1)} %bitcast.12), calls=%async_computation.2 | async-start | bytes 786432 | tf_op jit(solution)/shard_map/all_to_all | solution.py:134
  268.4 27.6 %all-to-all-done.2 = bf16[32,24,256]{2,1,0:T(8,128)(2,1)S(1)} async-done(((bf16[32,24,256]{2,1,0:T(8,128)(2,1)}), bf16[32,24,256]{2,1,0:T(8,128)(2,1)S(1)}, u32[]{:S(2)}, u32[]{:S(2)}) %all-to-all-start.2) | async-done | bytes 393248 | tf_op jit(solution)/shard_map/all_to_all | solution.py:134
  296.0 1.9 gather_fusion
  298.0 0.3 reshape.279
  298.2 0.7 multiply_reduce_fusion
  299.1 0.8 copy.35
  (49 shorter events, 2.0 us)
Async XLA Ops:
  6.5 244.9 %copy-start = (bf16[1,2048,256]{2,1,0:T(8,128)(2,1)S(1)}, bf16[1,2048,256]{2,1,0:T(8,128)(2,1)}, u32[]{:S(2)}) copy-start(bf16[1,2048,256]{2,1,0:T(8,128)(2,1)} %param.23) | copy-start | bytes 3145732
  6.5 22.9 %copy-start.2 = (s32[256,2]{0,1:T(2,128)S(1)}, s32[256,2]{0,1:T(2,128)}, u32[]{:S(2)}) copy-start(s32[256,2]{0,1:T(2,128)} %param.19) | copy-start | bytes 6148
  6.5 21.4 %copy-start.1 = (bf16[256,256]{1,0:T(8,128)(2,1)S(1)}, bf16[256,256]{1,0:T(8,128)(2,1)}, u32[]{:S(2)}) copy-start(bf16[256,256]{1,0:T(8,128)(2,1)} %param.12) | copy-start | bytes 393220
  7.4 8.8 %collective-permute-start.1 = (bf16[15]{0:T(256)(128)(2,1)S(1)}, bf16[15]{0:T(256)(128)(2,1)S(1)}, u32[]{:S(2)}, u32[]{:S(2)}) collective-permute-start(bf16[15]{0:T(256)(128)(2,1)S(1)} %slice.109), channel_id=1, source_target_pairs={{0,16},{16,32},{32,48},{48,64},{64,80},{80,96},{96,112},{112,128},... | collective-permute-start | bytes 98 | tf_op jit(solution)/shard_map/ppermute | solution.py:21
  13.0 5.1 %collective-permute-start = (bf16[15,128]{1,0:T(8,128)(2,1)S(1)}, bf16[15,128]{1,0:T(8,128)(2,1)S(1)}, u32[]{:S(2)}, u32[]{:S(2)}) collective-permute-start(bf16[15,128]{1,0:T(8,128)(2,1)S(1)} %slice.107), channel_id=1, source_target_pairs={{0,16},{16,32},{32,48},{48,64},{64,80},{80,96},{96,112},{112,128},... | collective-permute-start | bytes 11528 | tf_op jit(solution)/shard_map/ppermute | solution.py:21
  22.1 21.8 %all-to-all-start = ((bf16[16,256,128]{1,2,0:T(8,128)(2,1)}), bf16[16,256,128]{1,2,0:T(8,128)(2,1)S(1)}, u32[]{:S(2)}, u32[]{:S(2)}) async-start(bf16[16,256,128]{1,2,0:T(8,128)(2,1)} %broadcast_in_dim.8), calls=%async_computation | async-start | bytes 2097152 | tf_op jit(solution)/shard_map/all_to_all | solution.py:26
  27.7 152.1 %all-gather.3.cloned.1.call-start = ((), (), s32[]{:S(2)}) async-start(), calls=%async_computation.3 | async-start | bytes 6684672 | tf_op jit(solution)/shard_map/all_gather | solution.py:124
  43.9 140.8 %copy-start.5 = (bf16[1,4096,128]{2,1,0:T(8,128)(2,1)S(1)}, bf16[1,4096,128]{2,1,0:T(8,128)(2,1)}, u32[]{:S(2)}) copy-start(bf16[1,4096,128]{2,1,0:T(8,128)(2,1)} %param.22) | copy-start | bytes 3145732
  111.5 140.0 %all-gather.5.cloned.1.call-start = ((), (), s32[]{:S(2)}) async-start(), calls=%async_computation.4 | async-start | bytes 3932160 | tf_op jit(solution)/shard_map/all_gather | solution.py:49
  179.8 5.0 %copy-start.4 = (bf16[768,4096]{1,0:T(8,128)(2,1)S(1)}, bf16[768,4096]{1,0:T(8,128)(2,1)}, u32[]{:S(2)}) copy-start(bf16[768,4096]{1,0:T(8,128)(2,1)} %all-gather.3.cloned.1.call-done) | copy-start | bytes 18874372
  186.5 81.7 %copy-start.3 = (f32[256,2]{0,1:T(2,128)S(1)}, f32[256,2]{0,1:T(2,128)}, u32[]{:S(2)}) copy-start(f32[256,2]{0,1:T(2,128)} %param.20) | copy-start | bytes 6148
  255.1 40.9 %all-to-all-start.2 = ((bf16[32,24,256]{2,1,0:T(8,128)(2,1)}), bf16[32,24,256]{2,1,0:T(8,128)(2,1)S(1)}, u32[]{:S(2)}, u32[]{:S(2)}) async-start(bf16[32,24,256]{2,1,0:T(8,128)(2,1)} %bitcast.12), calls=%async_computation.2 | async-start | bytes 786432 | tf_op jit(solution)/shard_map/all_to_all | solution.py:134
Sparse Core Ops, SparseCore 0:
  111.6 68.1 all-gather.2
  202.4 48.9 all-gather.4
where the time goes:
time: 307 us
  waiting for transfers between devices  159 us (52%)
  blocking collectives  77.3 us (25%)
  starting transfers between devices  25.7 us (8%)
  matrix products  14.1 us (5%)
  between operations  13.7 us (4%)
  local copies, waits for them, and re-layouts  11.6 us (4%)
  other arithmetic  4.88 us (2%)
    all_gather x1, waiting for transfers between devices, shards(): piece = lax.all_gather(part_rows, TP, axis=1, tiled=True)  68.2 us
    all_gather x1, waiting for transfers between devices, whole_of(): whole = lax.all_gather(whole, axes[number], axis=dim, tiled=True)  49.1 us
    all_to_all x1, blocking collectives, shards(): lax.all_to_all(send.reshape(experts, slots_cap, cols), 'sp', split_axis=0...  48.2 us
    all_to_all x1, waiting for transfers between devices, shards(): lax.all_to_all(produced.reshape(n_sp, slots_cap, cols), 'sp', split_axis=...  27.6 us
    all_gather x1, blocking collectives, whole_of(): whole = lax.all_gather(whole, axes[number], axis=dim, tiled=True)  15.7 us
    psum x2, blocking collectives, by_axis(): return functools.reduce(lax.psum, axes, shard)  13.3 us
    all_to_all x1, waiting for transfers between devices, sent_to_all(): lax.all_to_all(jnp.broadcast_to(shard[None], (size, *shard.shape)), axis,...  13.3 us
    all_to_all x1, starting transfers between devices, shards(): lax.all_to_all(produced.reshape(n_sp, slots_cap, cols), 'sp', split_axis=...  13.2 us
  transfers between devices with their start and end apart: 6, of which 6 were waited for; matrix products, arithmetic and copies ran while one was open for 2% of the time, Pallas kernels for 0%

commit v1 on v0

v1 whole, which is shorter than its diff:
```python
import jax
import jax.numpy as jnp
from jax import lax
from jax.sharding import Mesh
from jax.sharding import PartitionSpec as P

TOPK = 2
SP = ("z", "c")
TP = ("y", "x")
EPS = 1e-06
F32 = jnp.float32
BF16 = jnp.bfloat16


def a2a(blocks, axis):
    return lax.all_to_all(blocks, axis, 0, 0, tiled=True)


def to_all(block, axis, size):
    return a2a(jnp.broadcast_to(block[None], (size, *block.shape)), axis)


def pool(pool_in, docs, pool_weight, pool_gain):
    length, width = pool_in.shape
    sp_index = lax.axis_index(SP)
    group = lax.axis_index(TP)
    size = lax.axis_size(SP)
    reach = 15
    tail = docs[length - 16 :].astype(BF16)
    edge = jnp.concatenate([pool_in[length - reach :], jnp.pad(tail, (0, width - 16))[None]], axis=0)
    prev = lax.ppermute(edge, SP, [(i, i + 1) for i in range(size - 1)])
    extended = jnp.concatenate([prev[:reach], pool_in], axis=0).astype(F32)
    own_docs = docs.astype(F32)
    ext_docs = jnp.concatenate([prev[reach, 1:16].astype(F32), own_docs])
    places = sp_index * length + jnp.arange(length)
    span = 2 ** (1 + group % 4)
    totals = jnp.zeros((length, width), F32)
    counts = jnp.zeros((length,), F32)
    for offset in range(16):
        shifted = extended[reach - offset : reach - offset + length]
        prior = ext_docs[reach - offset : reach - offset + length]
        same = ((places >= offset) & (prior == own_docs) & (offset < span)).astype(F32)
        totals = totals + same[:, None] * shifted
        counts = counts + same
    diff = (totals / counts[:, None] - extended[reach:]).astype(BF16)
    mixed = jnp.dot(diff, pool_weight[0], preferred_element_type=F32)
    return (mixed * pool_gain).astype(BF16)


def weights_of(w_gate, w_up, w_down, gain, gather, scatter):
    both = jnp.concatenate([w_gate, w_up], axis=1)
    if gather == "x":
        first = both.reshape(4, 1024, 256)
        own_gain = lax.dynamic_slice_in_dim(gain.reshape(4, 1024), lax.axis_index("y"), 1, 0)[0]
        second = w_down.reshape(4, 4, 128, 256).transpose(1, 0, 2, 3).reshape(4, 512, 256)
    else:
        first = both.reshape(4, 4, 256, 256).transpose(1, 0, 2, 3).reshape(4, 1024, 256)
        own_gain = lax.dynamic_slice_in_dim(gain.reshape(4, 4, 256), lax.axis_index("x"), 1, 1).reshape(1024)
        second = w_down.reshape(4, 512, 256)
    first = a2a(first, scatter)
    second = a2a(second, gather)
    first = (first.astype(F32) * own_gain[None, :, None]).astype(BF16)
    return first, second


def experts(rows, first, second, gather, scatter):
    count = rows.shape[0]
    got = to_all(rows, gather, 4)
    squares = jnp.sum(jnp.square(got.astype(F32)), axis=(0, 2))
    part = jnp.einsum("grf,sgfh->srh", got, first.reshape(4, 4, 256, 256), preferred_element_type=F32)
    parts = a2a(part.astype(BF16), scatter)
    all_squares = jnp.sum(to_all(squares.reshape(1, count), scatter, 4), axis=(0, 1))
    scale = lax.rsqrt(all_squares / 4096 + EPS)[:, None]
    both = jnp.sum(parts.astype(F32), axis=0) * scale
    gate, up = both[:, :128], both[:, 128:]
    act = (jax.nn.silu(gate) * up).astype(BF16)
    acts = to_all(act, scatter, 4)
    part = jnp.einsum("hrk,ghkf->grf", acts, second.reshape(4, 4, 128, 256), preferred_element_type=F32)
    parts = a2a(part.astype(BF16), gather)
    return jnp.sum(parts.astype(F32), axis=0).astype(BF16)


def shards(
    residual, pool_in, docs, pool_weight, pool_gain, out_weight, norm_gain, routes, route_weights, w_gate, w_up, w_down
):
    length, cols = residual.shape
    n_z, n_c = lax.axis_size("z"), lax.axis_size("c")
    n_exp = n_z * n_c
    cap = length * TOPK * 3 // (2 * n_exp)
    slots = n_exp * cap
    pooled = pool(pool_in, docs, pool_weight, pool_gain)
    ids = routes.reshape(-1)
    onehot = (ids[:, None] == jnp.arange(n_exp)[None, :]).astype(jnp.int32)
    rank = jnp.sum(onehot * (jnp.cumsum(onehot, axis=0) - 1), axis=1)
    place = (((ids % n_c) * n_z + ids // n_c) * cap + rank).reshape(length, TOPK)
    places = jnp.arange(slots)
    take = (place[:, 0][None, :] == places[:, None]) | (place[:, 1][None, :] == places[:, None])
    low = jnp.where(place[:, 0][:, None] == places[None, :], route_weights[:, 0][:, None], 0.0)
    mix = low + jnp.where(place[:, 1][:, None] == places[None, :], route_weights[:, 1][:, None], 0.0)
    mix_high = mix.astype(BF16)
    mix_low = (mix - mix_high.astype(F32)).astype(BF16)

    weights = {
        "x": weights_of(w_gate[0], w_up[0], w_down[0], norm_gain, "x", "y"),
        "y": weights_of(w_gate[0], w_up[0], w_down[0], norm_gain, "y", "x"),
    }

    pooled_all = to_all(pooled, TP, 16)
    proj = jnp.einsum("gtc,gcd->td", pooled_all, out_weight.reshape(16, 128, cols), preferred_element_type=F32)
    updated = (residual.astype(F32) + proj).astype(BF16)

    send = jnp.dot(take.astype(BF16), updated, preferred_element_type=F32).astype(BF16)
    send = a2a(send.reshape(n_c, n_z * cap, cols), "c")
    made = []
    for half, (gather, scatter) in enumerate((("x", "y"), ("y", "x"))):
        rows = a2a(send[half].reshape(n_z, cap, cols), "z").reshape(n_z * cap, cols)
        out = experts(rows, *weights[gather], gather, scatter)
        made.append(a2a(out.reshape(n_z, cap, cols), "z").reshape(n_z * cap, cols))
    back = a2a(jnp.stack(made), "c").reshape(slots, cols)
    summed = jnp.dot(mix_high, back, preferred_element_type=F32) + jnp.dot(
        mix_low, back, preferred_element_type=F32
    )
    return (updated.astype(F32) + summed).astype(BF16)


def solution(mesh):
    torus = Mesh(mesh.devices.reshape(-1, 2, 4, 4), ("z", "c", "y", "x"))
    in_specs = (
        P(SP, TP),
        P(SP, TP),
        P(SP),
        P(TP, None, None),
        P(TP),
        P(None, TP),
        P(),
        P(SP, None),
        P(SP, None),
        P(SP, None, TP),
        P(SP, None, TP),
        P(SP, None, TP),
    )
    return jax.shard_map(shards, mesh=torus, in_specs=in_specs, out_specs=P(SP, TP), check_vma=False)
```

time: 307 us -> 363 us (1.18)
  starting transfers between devices: 25.7 us -> 75.3 us
  other arithmetic: 4.88 us -> 18.5 us
  between operations: 13.7 us -> 0.53 us
  local copies, waits for them, and re-layouts: 11.6 us -> 15.4 us
  blocking collectives: 77.3 us -> 73.5 us
    all_gather x2 -> x0, waiting for transfers between devices: 117 us -> none  [the longest x1 68.2 us: shards(): piece = lax.all_gather(part_rows, TP, axis=1, tiled=True)]
    all_to_all x2 -> x17, waiting for transfers between devices: 40.9 us -> 158 us  [a2a(): return lax.all_to_all(blocks, axis, 0, 0, tiled=True)]
    all_to_all x2 -> x17, starting transfers between devices: 18.8 us -> 70.4 us  [a2a(): return lax.all_to_all(blocks, axis, 0, 0, tiled=True)]
    all_to_all x1 -> x4, blocking collectives: 48.2 us -> 73.5 us  [a2a(): return lax.all_to_all(blocks, axis, 0, 0, tiled=True)]
    all_gather x1 -> x0, blocking collectives: 15.7 us -> none  [whole_of(): whole = lax.all_gather(whole, axes[number], axis=dim, tiled=True)]
    psum x2 -> x0, blocking collectives: 13.3 us -> none  [by_axis(): return functools.reduce(lax.psum, axes, shard)]
    reduce_sum x1 -> x8, other arithmetic: 0.7 us -> 5.81 us  [the longest x2 2.73 us: experts(): squares = jnp.sum(jnp.square(got.astype(F32)), axis=(0, 2))]
    broadcast_in_dim x1 -> x8, local copies, waits for them, and re-layouts: 1.07 us -> 5.88 us  [the longest x7 5.88 us: to_all(): return a2a(jnp.broadcast_to(block[None], (size, *block.shape)), axis)]
  transfers between devices with their start and end apart: 6 -> 18, of which waited for: 6 -> 18; matrix products, arithmetic and copies ran while one was open for 2% -> 10% of each run, Pallas kernels for 0% -> 0%
where the time goes in v1:
time: 363 us; the launch traced here: 361 us
  waiting for transfers between devices  162 us (45%)
  starting transfers between devices  75.3 us (21%)
  blocking collectives  73.5 us (20%)
  other arithmetic  18.5 us (5%)
  local copies, waits for them, and re-layouts  15.4 us (4%)
  matrix products  15.4 us (4%)
    all_to_all x17, waiting for transfers between devices, a2a(): return lax.all_to_all(blocks, axis, 0, 0, tiled=True)  158 us
    all_to_all x4, blocking collectives, a2a(): return lax.all_to_all(blocks, axis, 0, 0, tiled=True)  73.5 us
    all_to_all x17, starting transfers between devices, a2a(): return lax.all_to_all(blocks, axis, 0, 0, tiled=True)  70.4 us
    dot_general x2, matrix products, experts(): jnp.einsum('grf,sgfh->srh', got, first.reshape(4, 4, 256, 256), preferred...  7.26 us
  transfers between devices with their start and end apart: 18, of which 18 were waited for; matrix products, arithmetic and copies ran while one was open for 10% of the time, Pallas kernels for 0%

profile of v1, /device:TPU:1, one launch (start us, length us, event | category | flops | bytes accessed | tf_op | source)
XLA Modules:
  0.0 360.6 jit_solution(2331898141214978496)
XLA Ops:
  1.6 4.9 %collective-permute-start = (bf16[16,128]{1,0:T(8,128)(2,1)S(1)}, bf16[16,128]{1,0:T(8,128)(2,1)S(1)}, u32[]{:S(2)}, u32[]{:S(2)}) collective-permute-start(bf16[16,128]{1,0:T(8,128)(2,1)S(1)} %pad_maximum_fusion.2), channel_id=1, source_target_pairs={{0,16},{16,32},{32,48},{48,64},{64,80},{80,96},{96,112},{112,128},... | collective-permute-start | bytes 12296 | tf_op jit(solution)/shard_map/ppermute | solution.py:31
  6.6 3.8 %collective-permute-done = bf16[16,128]{1,0:T(8,128)(2,1)S(1)} collective-permute-done((bf16[16,128]{1,0:T(8,128)(2,1)S(1)}, bf16[16,128]{1,0:T(8,128)(2,1)S(1)}, u32[]{:S(2)}, u32[]{:S(2)}) %collective-permute-start) | collective-permute-done | bytes 4128 | tf_op jit(solution)/shard_map/ppermute | solution.py:31
  15.2 3.7 %all-to-all-start = ((bf16[16,256,128]{2,1,0:T(8,128)(2,1)}), bf16[16,256,128]{2,1,0:T(8,128)(2,1)S(1)}, u32[]{:S(2)}, u32[]{:S(2)}) async-start(bf16[16,256,128]{2,1,0:T(8,128)(2,1)} %broadcast_in_dim.43), calls=%async_computation | async-start | bytes 2097152 | tf_op jit(solution)/shard_map/all_to_all | solution.py:16
  24.3 12.8 %all-to-all-done = bf16[16,256,128]{2,1,0:T(8,128)(2,1)S(1)} async-done(((bf16[16,256,128]{2,1,0:T(8,128)(2,1)}), bf16[16,256,128]{2,1,0:T(8,128)(2,1)S(1)}, u32[]{:S(2)}, u32[]{:S(2)}) %all-to-all-start) | async-done | bytes 1048608 | tf_op jit(solution)/shard_map/all_to_all | solution.py:16
  37.1 4.2 %all-to-all-start.8 = ((bf16[4,512,256]{2,1,0:T(8,128)(2,1)}), bf16[4,512,256]{2,1,0:T(8,128)(2,1)}, u32[]{:S(2)}, u32[]{:S(2)}) async-start(bf16[4,512,256]{2,1,0:T(8,128)(2,1)} %bitcast.22), calls=%async_computation.8 | async-start | bytes 2097152 | tf_op jit(solution)/shard_map/all_to_all | solution.py:16
  45.9 9.8 %all-to-all-done.8 = bf16[4,512,256]{2,1,0:T(8,128)(2,1)} async-done(((bf16[4,512,256]{2,1,0:T(8,128)(2,1)}), bf16[4,512,256]{2,1,0:T(8,128)(2,1)}, u32[]{:S(2)}, u32[]{:S(2)}) %all-to-all-start.8) | async-done | bytes 1048608 | tf_op jit(solution)/shard_map/all_to_all | solution.py:16
  55.7 5.5 %all_to_all.105 = bf16[2,384,256]{2,1,0:T(8,128)(2,1)S(1)} all-to-all(bf16[2,384,256]{2,1,0:T(8,128)(2,1)S(1)} %bitcast.129), channel_id=1, replica_groups=mesh['z'=16,'c'=2,'y'=4,'x'=4] {'c'}, dimensions={0} | all-to-all | bytes 786432 | tf_op jit(solution)/shard_map/all_to_all | solution.py:16
  61.2 3.6 %all-to-all-start.1 = ((bf16[4,1024,256]{2,1,0:T(8,128)(2,1)}), bf16[4,1024,256]{2,1,0:T(8,128)(2,1)S(1)}, u32[]{:S(2)}, u32[]{:S(2)}) async-start(bf16[4,1024,256]{2,1,0:T(8,128)(2,1)} %pad_maximum_fusion), calls=%async_computation.1 | async-start | bytes 4194304 | tf_op jit(solution)/shard_map/all_to_all | solution.py:16
  68.1 22.7 %all-to-all-done.1 = bf16[4,1024,256]{2,1,0:T(8,128)(2,1)S(1)} async-done(((bf16[4,1024,256]{2,1,0:T(8,128)(2,1)}), bf16[4,1024,256]{2,1,0:T(8,128)(2,1)S(1)}, u32[]{:S(2)}, u32[]{:S(2)}) %all-to-all-start.1) | async-done | bytes 2097184 | tf_op jit(solution)/shard_map/all_to_all | solution.py:16
  92.1 3.6 %all-to-all-start.11 = ((bf16[4,1024,256]{2,1,0:T(8,128)(2,1)}), bf16[4,1024,256]{2,1,0:T(8,128)(2,1)S(1)}, u32[]{:S(2)}, u32[]{:S(2)}) async-start(bf16[4,1024,256]{2,1,0:T(8,128)(2,1)} %bitcast.113), calls=%async_computation.11 | async-start | bytes 4194304 | tf_op jit(solution)/shard_map/all_to_all | solution.py:16
  96.6 24.4 %all-to-all-done.11 = bf16[4,1024,256]{2,1,0:T(8,128)(2,1)S(1)} async-done(((bf16[4,1024,256]{2,1,0:T(8,128)(2,1)}), bf16[4,1024,256]{2,1,0:T(8,128)(2,1)S(1)}, u32[]{:S(2)}, u32[]{:S(2)}) %all-to-all-start.11) | async-done | bytes 2097184 | tf_op jit(solution)/shard_map/all_to_all | solution.py:16
  120.9 27.4 %all_to_all.106 = bf16[16,24,256]{2,1,0:T(8,128)(2,1)S(1)} all-to-all(bf16[16,24,256]{2,1,0:T(8,128)(2,1)} %bitcast.124), channel_id=1, replica_groups=mesh['z'=16,'c'=2,'y'=4,'x'=4] {'z'}, dimensions={0} | all-to-all | bytes 393216 | tf_op jit(solution)/shard_map/all_to_all | solution.py:16
  148.3 19.6 %all_to_all.107 = bf16[16,24,256]{2,1,0:T(8,128)(2,1)S(1)} all-to-all(bf16[16,24,256]{2,1,0:T(8,128)(2,1)} %bitcast.123), channel_id=1, replica_groups=mesh['z'=16,'c'=2,'y'=4,'x'=4] {'z'}, dimensions={0} | all-to-all | bytes 393216 | tf_op jit(solution)/shard_map/all_to_all | solution.py:16
  168.9 4.2 %all-to-all-start.4 = ((bf16[4,384,256]{2,1,0:T(8,128)(2,1)}), bf16[4,384,256]{2,1,0:T(8,128)(2,1)}, u32[]{:S(2)}, u32[]{:S(2)}) async-start(bf16[4,384,256]{2,1,0:T(8,128)(2,1)} %broadcast_in_dim.50), calls=%async_computation.4 | async-start | bytes 1572864 | tf_op jit(solution)/shard_map/all_to_all | solution.py:16
  173.1 8.3 %all-to-all-done.4 = bf16[4,384,256]{2,1,0:T(8,128)(2,1)} async-done(((bf16[4,384,256]{2,1,0:T(8,128)(2,1)}), bf16[4,384,256]{2,1,0:T(8,128)(2,1)}, u32[]{:S(2)}, u32[]{:S(2)}) %all-to-all-start.4) | async-done | bytes 786464 | tf_op jit(solution)/shard_map/all_to_all | solution.py:16
  182.4 4.2 %all-to-all-start.13 = ((bf16[4,384,256]{2,1,0:T(8,128)(2,1)}), bf16[4,384,256]{2,1,0:T(8,128)(2,1)}, u32[]{:S(2)}, u32[]{:S(2)}) async-start(bf16[4,384,256]{2,1,0:T(8,128)(2,1)} %broadcast_in_dim.54), calls=%async_computation.13 | async-start | bytes 1572864 | tf_op jit(solution)/shard_map/all_to_all | solution.py:16
  191.3 3.7 %all-to-all-done.13 = bf16[4,384,256]{2,1,0:T(8,128)(2,1)} async-done(((bf16[4,384,256]{2,1,0:T(8,128)(2,1)}), bf16[4,384,256]{2,1,0:T(8,128)(2,1)}, u32[]{:S(2)}, u32[]{:S(2)}) %all-to-all-start.13) | async-done | bytes 786464 | tf_op jit(solution)/shard_map/all_to_all | solution.py:16
  206.8 3.9 %fusion.2 = bf16[4,384,256]{1,2,0:T(8,128)(2,1)} fusion(bf16[4,4,256,256]{3,2,1,0:T(8,128)(2,1)} %bitcast.118, bf16[4,384,256]{2,1,0:T(8,128)(2,1)} %all-to-all-done.4), kind=kOutput, calls=%fused_computation.14 | convolution fusion | flops 805699584 | bytes 3670016 | tf_op jit(solution)/shard_map/grf,sgfh->srh/dot_general | solution.py:70
  210.9 4.2 %all-to-all-start.5 = ((bf16[4,384,256]{1,2,0:T(8,128)(2,1)}), bf16[4,384,256]{1,2,0:T(8,128)(2,1)}, u32[]{:S(2)}, u32[]{:S(2)}) async-start(bf16[4,384,256]{1,2,0:T(8,128)(2,1)} %fusion.2), calls=%async_computation.5 | async-start | bytes 1572864 | tf_op jit(solution)/shard_map/all_to_all | solution.py:16
  218.8 4.7 %all-to-all-done.5 = bf16[4,384,256]{1,2,0:T(8,128)(2,1)} async-done(((bf16[4,384,256]{1,2,0:T(8,128)(2,1)}), bf16[4,384,256]{1,2,0:T(8,128)(2,1)}, u32[]{:S(2)}, u32[]{:S(2)}) %all-to-all-start.5) | async-done | bytes 786464 | tf_op jit(solution)/shard_map/all_to_all | solution.py:16
  223.5 4.0 %all-to-all-start.14 = ((bf16[4,384,256]{1,2,0:T(8,128)(2,1)}), bf16[4,384,256]{1,2,0:T(8,128)(2,1)S(1)}, u32[]{:S(2)}, u32[]{:S(2)}) async-start(bf16[4,384,256]{1,2,0:T(8,128)(2,1)} %fusion.3), calls=%async_computation.14 | async-start | bytes 1572864 | tf_op jit(solution)/shard_map/all_to_all | solution.py:16
  227.6 8.3 %all-to-all-done.14 = bf16[4,384,256]{1,2,0:T(8,128)(2,1)S(1)} async-done(((bf16[4,384,256]{1,2,0:T(8,128)(2,1)}), bf16[4,384,256]{1,2,0:T(8,128)(2,1)S(1)}, u32[]{:S(2)}, u32[]{:S(2)}) %all-to-all-start.14) | async-done | bytes 786464 | tf_op jit(solution)/shard_map/all_to_all | solution.py:16
  241.0 8.1 %all-to-all-done.17 = bf16[4,512,256]{2,1,0:T(8,128)(2,1)S(1)} async-done(((bf16[4,512,256]{2,1,0:T(8,128)(2,1)}), bf16[4,512,256]{2,1,0:T(8,128)(2,1)S(1)}, u32[]{:S(2)}, u32[]{:S(2)}) %all-to-all-start.17) | async-done | bytes 1048608 | tf_op jit(solution)/shard_map/all_to_all | solution.py:16
  253.6 8.4 %all-to-all-done.7 = bf16[4,384,128]{2,1,0:T(8,128)(2,1)S(1)} async-done(((bf16[4,384,128]{2,1,0:T(8,128)(2,1)}), bf16[4,384,128]{2,1,0:T(8,128)(2,1)S(1)}, u32[]{:S(2)}, u32[]{:S(2)}) %all-to-all-start.7) | async-done | bytes 393248 | tf_op jit(solution)/shard_map/all_to_all | solution.py:16
  277.4 6.8 %all-to-all-done.9 = bf16[4,384,256]{2,1,0:T(8,128)(2,1)S(1)} async-done(((bf16[4,384,256]{2,1,0:T(8,128)(2,1)}), bf16[4,384,256]{2,1,0:T(8,128)(2,1)S(1)}, u32[]{:S(2)}, u32[]{:S(2)}) %all-to-all-start.9) | async-done | bytes 786464 | tf_op jit(solution)/shard_map/all_to_all | solution.py:16
  284.2 4.7 %all-to-all-start.18 = ((bf16[4,384,256]{2,1,0:T(8,128)(2,1)}), bf16[4,384,256]{2,1,0:T(8,128)(2,1)S(1)}, u32[]{:S(2)}, u32[]{:S(2)}) async-start(bf16[4,384,256]{2,1,0:T(8,128)(2,1)} %fusion.1), calls=%async_computation.18 | async-start | bytes 1572864 | tf_op jit(solution)/shard_map/all_to_all | solution.py:16
  289.8 7.5 %all-to-all-done.18 = bf16[4,384,256]{2,1,0:T(8,128)(2,1)S(1)} async-done(((bf16[4,384,256]{2,1,0:T(8,128)(2,1)}), bf16[4,384,256]{2,1,0:T(8,128)(2,1)S(1)}, u32[]{:S(2)}, u32[]{:S(2)}) %all-to-all-start.18) | async-done | bytes 786464 | tf_op jit(solution)/shard_map/all_to_all | solution.py:16
  297.3 8.7 %all-to-all-start.10 = ((bf16[16,24,256]{2,1,0:T(8,128)(2,1)}), bf16[16,24,256]{2,1,0:T(8,128)(2,1)S(1)}, u32[]{:S(2)}, u32[]{:S(2)}) async-start(bf16[16,24,256]{2,1,0:T(8,128)(2,1)} %bitcast.27), calls=%async_computation.10 | async-start | bytes 393216 | tf_op jit(solution)/shard_map/all_to_all | solution.py:16
  306.9 11.5 %all-to-all-done.10 = bf16[16,24,256]{2,1,0:T(8,128)(2,1)S(1)} async-done(((bf16[16,24,256]{2,1,0:T(8,128)(2,1)}), bf16[16,24,256]{2,1,0:T(8,128)(2,1)S(1)}, u32[]{:S(2)}, u32[]{:S(2)}) %all-to-all-start.10) | async-done | bytes 196640 | tf_op jit(solution)/shard_map/all_to_all | solution.py:16
  318.3 4.8 %all-to-all-start.19 = ((bf16[16,24,256]{2,1,0:T(8,128)(2,1)}), bf16[16,24,256]{2,1,0:T(8,128)(2,1)S(1)}, u32[]{:S(2)}, u32[]{:S(2)}) async-start(bf16[16,24,256]{2,1,0:T(8,128)(2,1)} %bitcast.47), calls=%async_computation.19 | async-start | bytes 393216 | tf_op jit(solution)/shard_map/all_to_all | solution.py:16
  323.2 14.9 %all-to-all-done.19 = bf16[16,24,256]{2,1,0:T(8,128)(2,1)S(1)} async-done(((bf16[16,24,256]{2,1,0:T(8,128)(2,1)}), bf16[16,24,256]{2,1,0:T(8,128)(2,1)S(1)}, u32[]{:S(2)}, u32[]{:S(2)}) %all-to-all-start.19) | async-done | bytes 196640 | tf_op jit(solution)/shard_map/all_to_all | solution.py:16
  338.1 21.0 %all_to_all.108 = bf16[2,384,256]{2,1,0:T(8,128)(2,1)S(1)} all-to-all(bf16[2,384,256]{2,1,0:T(8,128)(2,1)S(1)} %pad_maximum_fusion.1), channel_id=1, replica_groups=mesh['z'=16,'c'=2,'y'=4,'x'=4] {'c'}, dimensions={0} | all-to-all | bytes 786432 | tf_op jit(solution)/shard_map/all_to_all | solution.py:16
  (104 shorter events, 72.1 us)
Async XLA Ops:
  0.0 44.5 %copy-start = (bf16[2048,256]{1,0:T(8,128)(2,1)S(1)}, bf16[2048,256]{1,0:T(8,128)(2,1)}, u32[]{:S(2)}) copy-start(bf16[2048,256]{1,0:T(8,128)(2,1)} %param.17) | copy-start | bytes 3145732
  1.6 8.8 %collective-permute-start = (bf16[16,128]{1,0:T(8,128)(2,1)S(1)}, bf16[16,128]{1,0:T(8,128)(2,1)S(1)}, u32[]{:S(2)}, u32[]{:S(2)}) collective-permute-start(bf16[16,128]{1,0:T(8,128)(2,1)S(1)} %pad_maximum_fusion.2), channel_id=1, source_target_pairs={{0,16},{16,32},{32,48},{48,64},{64,80},{80,96},{96,112},{112,128},... | collective-permute-start | bytes 12296 | tf_op jit(solution)/shard_map/ppermute | solution.py:31
  14.0 4.9 %copy-start.8 = (s32[256,2]{0,1:T(2,128)S(1)}, s32[256,2]{0,1:T(2,128)}, u32[]{:S(2)}) copy-start(s32[256,2]{0,1:T(2,128)} %param.19) | copy-start | bytes 6148
  15.2 22.0 %all-to-all-start = ((bf16[16,256,128]{2,1,0:T(8,128)(2,1)}), bf16[16,256,128]{2,1,0:T(8,128)(2,1)S(1)}, u32[]{:S(2)}, u32[]{:S(2)}) async-start(bf16[16,256,128]{2,1,0:T(8,128)(2,1)} %broadcast_in_dim.43), calls=%async_computation | async-start | bytes 2097152 | tf_op jit(solution)/shard_map/all_to_all | solution.py:16
  21.8 2.4 copy-start.6
  21.8 19.8 %copy-start.2 = (bf16[1,4096,128]{2,1,0:T(8,128)(2,1)S(1)}, bf16[1,4096,128]{2,1,0:T(8,128)(2,1)}, u32[]{:S(2)}) copy-start(bf16[1,4096,128]{2,1,0:T(8,128)(2,1)} %param.22) | copy-start | bytes 3145732
  37.1 18.5 %all-to-all-start.8 = ((bf16[4,512,256]{2,1,0:T(8,128)(2,1)}), bf16[4,512,256]{2,1,0:T(8,128)(2,1)}, u32[]{:S(2)}, u32[]{:S(2)}) async-start(bf16[4,512,256]{2,1,0:T(8,128)(2,1)} %bitcast.22), calls=%async_computation.8 | async-start | bytes 2097152 | tf_op jit(solution)/shard_map/all_to_all | solution.py:16
  41.6 3.3 copy-start.10
  41.6 3.3 copy-start.12
  41.6 2.8 copy-start.3
  44.9 0.7 copy-start.4
  61.2 29.6 %all-to-all-start.1 = ((bf16[4,1024,256]{2,1,0:T(8,128)(2,1)}), bf16[4,1024,256]{2,1,0:T(8,128)(2,1)S(1)}, u32[]{:S(2)}, u32[]{:S(2)}) async-start(bf16[4,1024,256]{2,1,0:T(8,128)(2,1)} %pad_maximum_fusion), calls=%async_computation.1 | async-start | bytes 4194304 | tf_op jit(solution)/shard_map/all_to_all | solution.py:16
  90.8 1.3 copy-start.1
  92.1 28.8 %all-to-all-start.11 = ((bf16[4,1024,256]{2,1,0:T(8,128)(2,1)}), bf16[4,1024,256]{2,1,0:T(8,128)(2,1)S(1)}, u32[]{:S(2)}, u32[]{:S(2)}) async-start(bf16[4,1024,256]{2,1,0:T(8,128)(2,1)} %bitcast.113), calls=%async_computation.11 | async-start | bytes 4194304 | tf_op jit(solution)/shard_map/all_to_all | solution.py:16
  95.8 77.3 %copy-start.7 = (f32[4096]{0:T(1024)S(1)}, f32[4096]{0:T(1024)}, u32[]{:S(2)}) copy-start(f32[4096]{0:T(1024)} %param.18) | copy-start | bytes 49156
  168.9 12.6 %all-to-all-start.4 = ((bf16[4,384,256]{2,1,0:T(8,128)(2,1)}), bf16[4,384,256]{2,1,0:T(8,128)(2,1)}, u32[]{:S(2)}, u32[]{:S(2)}) async-start(bf16[4,384,256]{2,1,0:T(8,128)(2,1)} %broadcast_in_dim.50), calls=%async_computation.4 | async-start | bytes 1572864 | tf_op jit(solution)/shard_map/all_to_all | solution.py:16
  182.4 12.6 %all-to-all-start.13 = ((bf16[4,384,256]{2,1,0:T(8,128)(2,1)}), bf16[4,384,256]{2,1,0:T(8,128)(2,1)}, u32[]{:S(2)}, u32[]{:S(2)}) async-start(bf16[4,384,256]{2,1,0:T(8,128)(2,1)} %broadcast_in_dim.54), calls=%async_computation.13 | async-start | bytes 1572864 | tf_op jit(solution)/shard_map/all_to_all | solution.py:16
  195.6 7.3 %all-to-all-start.6 = ((f32[4,1,384]{2,1,0:T(1,128)}), f32[4,1,384]{2,1,0:T(1,128)S(1)}, u32[]{:S(2)}, u32[]{:S(2)}) async-start(f32[4,1,384]{2,1,0:T(1,128)} %broadcast_in_dim.51), calls=%async_computation.6 | async-start | bytes 12288 | tf_op jit(solution)/shard_map/all_to_all | solution.py:16
  203.6 7.4 %all-to-all-start.15 = ((f32[4,1,384]{2,1,0:T(1,128)}), f32[4,1,384]{2,1,0:T(1,128)S(1)}, u32[]{:S(2)}, u32[]{:S(2)}) async-start(f32[4,1,384]{2,1,0:T(1,128)} %broadcast_in_dim.55), calls=%async_computation.15 | async-start | bytes 12288 | tf_op jit(solution)/shard_map/all_to_all | solution.py:16
  210.9 12.6 %all-to-all-start.5 = ((bf16[4,384,256]{1,2,0:T(8,128)(2,1)}), bf16[4,384,256]{1,2,0:T(8,128)(2,1)}, u32[]{:S(2)}, u32[]{:S(2)}) async-start(bf16[4,384,256]{1,2,0:T(8,128)(2,1)} %fusion.2), calls=%async_computation.5 | async-start | bytes 1572864 | tf_op jit(solution)/shard_map/all_to_all | solution.py:16
  223.5 12.4 %all-to-all-start.14 = ((bf16[4,384,256]{1,2,0:T(8,128)(2,1)}), bf16[4,384,256]{1,2,0:T(8,128)(2,1)S(1)}, u32[]{:S(2)}, u32[]{:S(2)}) async-start(bf16[4,384,256]{1,2,0:T(8,128)(2,1)} %fusion.3), calls=%async_computation.14 | async-start | bytes 1572864 | tf_op jit(solution)/shard_map/all_to_all | solution.py:16
  235.9 13.2 %all-to-all-start.17 = ((bf16[4,512,256]{2,1,0:T(8,128)(2,1)}), bf16[4,512,256]{2,1,0:T(8,128)(2,1)S(1)}, u32[]{:S(2)}, u32[]{:S(2)}) async-start(bf16[4,512,256]{2,1,0:T(8,128)(2,1)} %bitcast.42), calls=%async_computation.17 | async-start | bytes 2097152 | tf_op jit(solution)/shard_map/all_to_all | solution.py:16
  249.9 12.1 %all-to-all-start.7 = ((bf16[4,384,128]{2,1,0:T(8,128)(2,1)}), bf16[4,384,128]{2,1,0:T(8,128)(2,1)S(1)}, u32[]{:S(2)}, u32[]{:S(2)}) async-start(bf16[4,384,128]{2,1,0:T(8,128)(2,1)} %broadcast_in_dim.52), calls=%async_computation.7 | async-start | bytes 786432 | tf_op jit(solution)/shard_map/all_to_all | solution.py:16
  262.8 9.7 %all-to-all-start.16 = ((bf16[4,384,128]{2,1,0:T(8,128)(2,1)}), bf16[4,384,128]{2,1,0:T(8,128)(2,1)S(1)}, u32[]{:S(2)}, u32[]{:S(2)}) async-start(bf16[4,384,128]{2,1,0:T(8,128)(2,1)} %broadcast_in_dim.56), calls=%async_computation.16 | async-start | bytes 786432 | tf_op jit(solution)/shard_map/all_to_all | solution.py:16
  272.4 11.8 %all-to-all-start.9 = ((bf16[4,384,256]{2,1,0:T(8,128)(2,1)}), bf16[4,384,256]{2,1,0:T(8,128)(2,1)S(1)}, u32[]{:S(2)}, u32[]{:S(2)}) async-start(bf16[4,384,256]{2,1,0:T(8,128)(2,1)} %fusion), calls=%async_computation.9 | async-start | bytes 1572864 | tf_op jit(solution)/shard_map/all_to_all | solution.py:16
  277.4 45.7 %copy-start.9 = (f32[256,2]{0,1:T(2,128)S(1)}, f32[256,2]{0,1:T(2,128)}, u32[]{:S(2)}) copy-start(f32[256,2]{0,1:T(2,128)} %param.20) | copy-start | bytes 6148
  284.2 13.1 %all-to-all-start.18 = ((bf16[4,384,256]{2,1,0:T(8,128)(2,1)}), bf16[4,384,256]{2,1,0:T(8,128)(2,1)S(1)}, u32[]{:S(2)}, u32[]{:S(2)}) async-start(bf16[4,384,256]{2,1,0:T(8,128)(2,1)} %fusion.1), calls=%async_computation.18 | async-start | bytes 1572864 | tf_op jit(solution)/shard_map/all_to_all | solution.py:16
  289.0 70.2 %copy-start.11 = (s32[256]{0:T(256)S(1)}, s32[256]{0:T(256)}, u32[]{:S(2)}) copy-start(s32[256]{0:T(256)} %copy-done.10) | copy-start | bytes 3076
  289.0 70.2 %copy-start.13 = (s32[256]{0:T(256)S(1)}, s32[256]{0:T(256)}, u32[]{:S(2)}) copy-start(s32[256]{0:T(256)} %copy-done.12) | copy-start | bytes 3076
  297.3 21.0 %all-to-all-start.10 = ((bf16[16,24,256]{2,1,0:T(8,128)(2,1)}), bf16[16,24,256]{2,1,0:T(8,128)(2,1)S(1)}, u32[]{:S(2)}, u32[]{:S(2)}) async-start(bf16[16,24,256]{2,1,0:T(8,128)(2,1)} %bitcast.27), calls=%async_computation.10 | async-start | bytes 393216 | tf_op jit(solution)/shard_map/all_to_all | solution.py:16
  306.9 52.7 %copy-start.5 = (bf16[256,256]{1,0:T(8,128)(2,1)S(1)}, bf16[256,256]{1,0:T(8,128)(2,1)}, u32[]{:S(2)}) copy-start(bf16[256,256]{1,0:T(8,128)(2,1)} %copy-done.4) | copy-start | bytes 393220
  318.3 19.7 %all-to-all-start.19 = ((bf16[16,24,256]{2,1,0:T(8,128)(2,1)}), bf16[16,24,256]{2,1,0:T(8,128)(2,1)S(1)}, u32[]{:S(2)}, u32[]{:S(2)}) async-start(bf16[16,24,256]{2,1,0:T(8,128)(2,1)} %bitcast.47), calls=%async_computation.19 | async-start | bytes 393216 | tf_op jit(solution)/shard_map/all_to_all | solution.py:16
